TPU v7x, 512 devices: a 4x2x32 block of a 4x8x32 slice. The times are simulated.
512 devices in a mesh: grp: 2 (over y), sp: 64 (over z, core), tp: 4 (over x).
Axes of the slice: x: 4, y: 2, z: 32, core: 2. Of those that a mesh axis runs over, the one named last changes fastest.
The devices are a block of a 4x8x32 slice.
Arguments:
- recurrent_query: bfloat16 [32768, 1024], P(('grp', 'sp'), 'tp'), parts along dimension 0, may hold values from -6 to 6
- recurrent_forget_gate: bfloat16 [32768, 1024], P(('grp', 'sp'), 'tp'), parts along dimension 0, may hold values from -4.5 to 4.5
- recurrent_value: bfloat16 [32768, 1024], P(('grp', 'sp'), 'tp'), parts along dimension 0, may hold values from -6 to 6
- recurrent_gate_lower_bound: float32 [1024], P('tp'), may hold values from 1.5 to 14
- recurrent_added_decay: float32 [32768, 8], P(('grp', 'sp'), 'tp'), parts along dimension 0, may hold values from -0.51 to 0
- recurrent_norm_gain: float32 [128], replicated, may hold values from 0.1 to 1.9
- attention_query_first: bfloat16 [32768, 512], P(('grp', 'sp'), 'tp'), parts along dimension 0, may hold values from -20 to 20
- attention_key_first: bfloat16 [32768, 256], P(('grp', 'sp'), 'tp'), parts along dimension 0, may hold values from -20 to 20
- attention_query_second: bfloat16 [32768, 512], P(('grp', 'sp'), 'tp'), parts along dimension 0, may hold values from -20 to 20
- attention_key_second: bfloat16 [32768, 256], P(('grp', 'sp'), 'tp'), parts along dimension 0, may hold values from -20 to 20
- attention_value: bfloat16 [32768, 512], P(('grp', 'sp'), 'tp'), parts along dimension 0, may hold values from -6 to 6
- second_map_weight: float32 [8], P('tp'), may hold values from 0.3 to 0.8
- attention_norm_gain: float32 [128], replicated, may hold values from 0.1 to 1.9
- output_weight: bfloat16 [2, 1024, 2048], P(None, 'tp', 'sp'), may hold values from -0.125 to 0.125
Outputs:
- mixed: bfloat16 [32768, 2048], P(('grp', 'sp', 'tp')), parts along dimension 0
There are 2 independent parts, one for each index of `grp`. A program takes and returns all parts, laid end to end along the dimension named above; an argument that names none is the same for every part. Nothing has to cross between parts.
All inputs are finite; a program needn't handle non-finite values.
Results may differ from a plain program's by a relative error of at most 0.02.
Values may be sent and summed in bfloat16 or wider, within the bound.
A program may use at most 64 MiB of HBM per device.

v0:
```python
import jax
import jax.numpy as jnp
from jax import lax
from jax.sharding import PartitionSpec as P

HG_DK = 128
HG_DV = 128
DA_HD = 64
BLK = 32
epsilon = 1e-06
key_span = 512


def carried_in(array, axis, combine, identity):
    size, place = (lax.axis_size(axis), lax.axis_index(axis))
    everything = jax.tree.map(
        lambda part, kind: lax.all_gather(part.astype(kind), axis),
        array,
        (jnp.bfloat16, jnp.bfloat16),
    )
    start = jax.tree.map(
        lambda part, zero: jnp.broadcast_to(jnp.asarray(zero, part.dtype), part.shape),
        array,
        identity,
    )

    def hop(k, before):
        reached = k < place
        new = combine(
            before, jax.tree.map(lambda part, own: part[k].astype(own.dtype), everything, array)
        )
        return jax.tree.map(lambda a, b: jnp.where(reached, a, b), new, before)

    return lax.fori_loop(0, size, hop, start)


def in_one_piece(arrays, axis, dim, along):
    ends, at = ([], 0)
    for a in arrays[:-1]:
        at += a.shape[along]
        ends.append(at)
    both = jnp.concatenate(arrays, axis=along)
    return tuple(jnp.split(lax.all_gather(both, axis, axis=dim, tiled=True), ends, axis=along))


def split_up(array, dim, size):
    before, after = (array.shape[:dim], array.shape[dim + 1 :])
    return jnp.moveaxis(array.reshape(*before, size, -1, *after), dim, 0)


def summed_on_arrival(array, axis, dim):
    size = lax.axis_size(axis)
    pieces = lax.all_to_all(split_up(array, dim, size), axis, 0, 0, tiled=True)
    return jnp.sum(pieces.astype(jnp.float32), axis=0)


def head_norm(head_values, gain_vec):
    mean_square = jnp.mean(head_values * head_values, axis=-1, keepdims=True)
    return head_values * lax.rsqrt(mean_square + epsilon) * gain_vec


def decay_factors(gate_preactivation, lower_bound_logit, added_log_decay, number_of_heads):
    token_count = gate_preactivation.shape[0]
    floor_rate = jax.nn.sigmoid(-lower_bound_logit).reshape(number_of_heads, -1)
    state_inflow = floor_rate[None] * jax.nn.sigmoid(
        -gate_preactivation.astype(jnp.float32)
    ).reshape(token_count, number_of_heads, -1)
    decay_logarithm = jnp.log1p(-state_inflow) + added_log_decay[:, :, None]
    return (state_inflow, decay_logarithm)


def recurrence_blocks(queries, decay_logarithm, state_inflow, value_rows, block_len):
    token_count, number_of_heads, key_width = queries.shape
    block_count = token_count // block_len

    def to_blocks(source):
        return source.reshape(block_count, block_len, number_of_heads, source.shape[-1])

    causal = jnp.tril(jnp.ones((block_len, block_len), jnp.float32))[:, :, None, None]

    def block_step(carry_state, inputs):
        query_blk, decay_blk, inflow_blk, value_blk = inputs
        cumulative = jnp.cumsum(decay_blk, axis=0)
        relative = cumulative[:, None] - cumulative[None, :]
        decay_table = jnp.exp(jnp.minimum(relative, 0.0)) * causal
        scores = jnp.einsum("thd,shd,tshd->hts", query_blk, inflow_blk, decay_table)
        block_out = jnp.einsum("hts,shv->thv", scores, value_blk)
        block_out = block_out + jnp.einsum(
            "thd,hdv->thv", query_blk * jnp.exp(cumulative), carry_state
        )
        last_log = cumulative[-1]
        new_state = jnp.exp(last_log)[:, :, None] * carry_state + jnp.einsum(
            "shd,shv->hdv", inflow_blk * jnp.exp(last_log[None] - cumulative), value_blk
        )
        return (new_state, block_out)

    zero_state = jnp.zeros((number_of_heads, key_width, value_rows.shape[-1]), jnp.float32)
    final_state, outputs = lax.scan(
        block_step,
        zero_state,
        (
            to_blocks(queries),
            to_blocks(decay_logarithm),
            to_blocks(state_inflow),
            to_blocks(value_rows),
        ),
    )
    return (final_state, outputs.reshape(token_count, number_of_heads, -1))


def chain_pair(earlier, following):
    return (earlier[0] * following[0], following[0][:, :, None] * earlier[1] + following[1])


def recurrent_path_output(
    recurrent_query,
    recurrent_forget_gate,
    recurrent_value,
    recurrent_gate_lower_bound,
    recurrent_added_decay,
    recurrent_norm_gain,
):
    token_count = recurrent_query.shape[0]
    number_of_heads = recurrent_gate_lower_bound.shape[0] // HG_DK
    state_inflow, decay_logarithm = decay_factors(
        recurrent_forget_gate, recurrent_gate_lower_bound, recurrent_added_decay, number_of_heads
    )
    queries = recurrent_query.astype(jnp.float32).reshape(token_count, number_of_heads, HG_DK)
    value_rows = recurrent_value.astype(jnp.float32).reshape(token_count, number_of_heads, HG_DV)
    final_state, local_out = recurrence_blocks(
        queries, decay_logarithm, state_inflow, value_rows, BLK
    )
    running_log = jnp.cumsum(decay_logarithm, axis=0)
    through = jnp.exp(running_log[-1])
    incoming = carried_in(
        (through, final_state),
        "sp",
        chain_pair,
        (jnp.ones_like(through), jnp.zeros_like(final_state)),
    )
    carried = jnp.einsum("thd,hdv->thv", queries * jnp.exp(running_log), incoming[1])
    return (
        head_norm(local_out + carried, recurrent_norm_gain)
        .astype(jnp.bfloat16)
        .reshape(token_count, -1)
    )


def attention_branch(
    attention_query_first,
    attention_key_first,
    attention_query_second,
    attention_key_second,
    attention_value,
    second_map_weight,
    attention_norm_gain,
):
    query_rows = attention_query_first.shape[0]
    key_heads = attention_key_first.shape[1] // DA_HD
    group_size = attention_query_first.shape[1] // DA_HD // key_heads
    score_scale = DA_HD ** (-0.5)
    offset = lax.axis_index("sp") * query_rows
    query_pos = offset + jnp.arange(query_rows)
    last_query = offset + query_rows - 1
    queries_one = attention_query_first.reshape(query_rows, key_heads, group_size, DA_HD)
    queries_two = attention_query_second.reshape(query_rows, key_heads, group_size, DA_HD)

    def map_update(running, queries, key_rows, value_rows, allowed):
        row_max, weight_mass, value_sum = running
        scores = (
            jnp.einsum("qkgd,skd->kgqs", queries, key_rows, preferred_element_type=jnp.float32)
            * score_scale
        )
        scores = jnp.where(allowed, scores, -1e30)
        new_max = jnp.maximum(row_max, jnp.max(scores, axis=-1))
        weights = jnp.where(allowed, jnp.exp(scores - new_max[..., None]), 0.0)
        shrink = jnp.exp(row_max - new_max)
        weight_mass = weight_mass * shrink + jnp.sum(weights, axis=-1)
        value_sum = value_sum * shrink[..., None] + jnp.einsum(
            "plew,wpd->pled",
            weights.astype(jnp.bfloat16),
            value_rows,
            preferred_element_type=jnp.float32,
        )
        return (new_max, weight_mass, value_sum)

    def key_block(running, block_one, block_two, block_values, first_row):
        span_rows = block_one.shape[0]
        key_pos = first_row + jnp.arange(span_rows)
        allowed = key_pos[None, :] <= query_pos[:, None]
        shaped_one = block_one.reshape(span_rows, key_heads, DA_HD)
        shaped_two = block_two.reshape(span_rows, key_heads, DA_HD)
        shaped_values = block_values.reshape(span_rows, key_heads, 2 * DA_HD)
        return (
            map_update(running[0], queries_one, shaped_one, shaped_values, allowed),
            map_update(running[1], queries_two, shaped_two, shaped_values, allowed),
        )

    def guarded_block(running, block_one, block_two, block_values, first_row):

        def compute(state_in):
            return key_block(state_in, block_one, block_two, block_values, first_row)

        def unchanged(state_in):
            return state_in

        result = lax.cond(first_row > last_query, unchanged, compute, running)
        return result

    start_max = jnp.full((key_heads, group_size, query_rows), -1e30, jnp.float32)
    zero_mass = jnp.zeros((key_heads, group_size, query_rows), jnp.float32)
    zero_sum = jnp.zeros((key_heads, group_size, query_rows, 2 * DA_HD), jnp.float32)
    fresh_state = (start_max, zero_mass, zero_sum)
    running = (fresh_state, fresh_state)
    shard_one, shard_two, shard_values = in_one_piece(
        (attention_key_first, attention_key_second, attention_value), "sp", 0, 1
    )
    row_count = shard_one.shape[0]
    span_rows = min(row_count, key_span)
    full_count = row_count // span_rows

    def span_step(span_index, state_in):
        begin_row = span_index * span_rows
        return guarded_block(
            state_in,
            lax.dynamic_slice_in_dim(shard_one, begin_row, span_rows, 0),
            lax.dynamic_slice_in_dim(shard_two, begin_row, span_rows, 0),
            lax.dynamic_slice_in_dim(shard_values, begin_row, span_rows, 0),
            begin_row,
        )

    running = lax.fori_loop(0, full_count, span_step, running)
    first_map, second_map = running
    lambda_table = second_map_weight.reshape(key_heads, group_size)[:, :, None, None]
    combined = first_map[2] / first_map[1][..., None] - lambda_table * (
        second_map[2] / second_map[1][..., None]
    )
    combined = jnp.transpose(combined, (2, 0, 1, 3)).reshape(
        query_rows, key_heads * group_size, 2 * DA_HD
    )
    return head_norm(combined, attention_norm_gain).astype(jnp.bfloat16).reshape(query_rows, -1)


def shards(
    recurrent_query,
    recurrent_forget_gate,
    recurrent_value,
    recurrent_gate_lower_bound,
    recurrent_added_decay,
    recurrent_norm_gain,
    attention_query_first,
    attention_key_first,
    attention_query_second,
    attention_key_second,
    attention_value,
    second_map_weight,
    attention_norm_gain,
    output_weight,
):
    attended = attention_branch(
        attention_query_first,
        attention_key_first,
        attention_query_second,
        attention_key_second,
        attention_value,
        second_map_weight,
        attention_norm_gain,
    )
    recurrent_output = recurrent_path_output(
        recurrent_query,
        recurrent_forget_gate,
        recurrent_value,
        recurrent_gate_lower_bound,
        recurrent_added_decay,
        recurrent_norm_gain,
    )
    pieces = lax.all_gather(output_weight, "sp", axis=2, tiled=True)
    partial_terms = jnp.dot(
        recurrent_output, pieces[0], preferred_element_type=jnp.float32
    ) + jnp.dot(attended, pieces[1], preferred_element_type=jnp.float32)
    return summed_on_arrival(partial_terms.astype(jnp.bfloat16), "tp", 0).astype(jnp.bfloat16)


def solution(mesh):
    return jax.shard_map(
        shards,
        mesh=mesh,
        in_specs=(
            P(("grp", "sp"), "tp"),
            P(("grp", "sp"), "tp"),
            P(("grp", "sp"), "tp"),
            P("tp"),
            P(("grp", "sp"), "tp"),
            P(),
            P(("grp", "sp"), "tp"),
            P(("grp", "sp"), "tp"),
            P(("grp", "sp"), "tp"),
            P(("grp", "sp"), "tp"),
            P(("grp", "sp"), "tp"),
            P("tp"),
            P(),
            P(None, "tp", "sp"),
        ),
        out_specs=P(("grp", "sp", "tp"), None),
        check_vma=False,
    )
```

profile of v0, /device:TPU:2016, one launch (start us, length us, event | category | flops | bytes accessed | tf_op | source)
XLA Modules:
  0.0 664.5 jit_solution(9917278042523082611)
XLA Ops:
  11.3 21.9 %while.52 = (s32[]{:T(128)}, f32[2,128,128]{2,1,0:T(8,128)S(1)}, f32[8,32,2,128]{3,1,0,2:T(8,128)S(1)}, f32[8,32,2,128]{3,2,1,0:T(2,128)S(1)}, f32[8,32,2,128]{3...) while((s32[]{:T(128)}, f32[2,128,128]{2,1,0:T(8,128)S(1)}, ...), condition=%wide.region_2.3_spmd.clone, body=%wide.region_0.2_spmd.clone.sunk | while | flops 6725635 | bytes 3266684 | solution.py:98
  36.9 51.6 %all_gather.16 = bf16[64,2,128]{2,1,0:T(2,128)(2,1)S(1)} all-gather(bf16[1,2,128]{2,1,0:T(2,128)(2,1)S(1)} %fusion.67), channel_id=1, replica_groups=mesh['grp'=2,'sp'=64,'tp'=4] {'sp'}, dimensions={0}, use_global_device_ids=true | all-gather | bytes 33280 | tf_op jit(solution)/shard_map/all_gather | solution.py:17
  89.2 64.9 %all-gather.9.cloned.1.call-done = bf16[128,128,128]{2,1,0:T(8,128)(2,1)} async-done(((bf16[2,128,128]{2,1,0:T(8,128)(2,1)}), bf16[128,128,128]{2,1,0:T(8,128)(2,1)}) %all-gather.9.cloned.1.call-update) | async-done | bytes 4194320 | tf_op jit(solution)/shard_map/all_gather | solution.py:17
  154.1 64.9 %while.53 = (s32[]{:T(128)}, f32[2,128,128]{2,1,0:T(8,128)S(1)}, s32[]{:T(128)}, bf16[64,2,128]{2,1,0:T(2,128)(2,1)S(1)}, bf16[64,2,128,128]{3,2,1,0:T(8,128)(2,1)}, /*index=5*/s32[]{:T(128)}, s32[]{:T(128)}) while((s32[]{:T(128)}, f32[2,128,128]{2,1,0:T(8,128)S(1)}, s32[]{:T(128)}, bf16[64,2,128]{2,1,0:T(2,128)(2,1)S(1)}, ...), condition=%wide.region_6.0_spmd.clone, body=%wide.region_5.6_spmd.clone.sunk | while | flops 164100 | bytes 330345 | solution.py:34
  219.4 63.2 %all-gather.5.cloned.1.call-done = bf16[2,256,2048]{1,2,0:T(8,128)(2,1)} async-done(((bf16[2,256,32]{1,2,0:T(8,128)(2,1)}), bf16[2,256,2048]{1,2,0:T(8,128)(2,1)}) %all-gather.5.cloned.1.call-update) | async-done | bytes 2097168 | tf_op jit(solution)/shard_map/all_gather | solution.py:277
  284.2 148.2 %all-gather.7.cloned.1.call-done = bf16[16384,256]{0,1:T(8,128)(2,1)} async-done(((bf16[256,256]{0,1:T(8,128)(2,1)}), bf16[16384,256]{0,1:T(8,128)(2,1)}) %all-gather.7.cloned.1.call-update) | async-done | bytes 8388624 | tf_op jit(solution)/shard_map/all_gather | solution.py:43
  436.9 6.3 copy.178
  447.9 187.3 %while.51 = (s32[]{:T(128)}, f32[1,2,256]{2,1,0:T(2,128)S(1)}, f32[1,2,256]{2,1,0:T(2,128)S(1)}, f32[1,2,256,128]{3,2,1,0:T(8,128)S(1)}, f32[1,2,256]{2,1,0:T(2,...) while((s32[]{:T(128)}, f32[1,2,256]{2,1,0:T(2,128)S(1)}, ...), condition=%wide.region_15.16_spmd.clone, body=%wide.region_8.15_spmd.clone.sunk | while | flops 206442240 | bytes 8724921 | solution.py:232
  448.0 5.8 conditional.3
  453.8 5.8 conditional.3
  459.7 5.8 conditional.3
  465.5 5.8 conditional.3
  471.4 5.8 conditional.3
  477.2 5.8 conditional.3
  483.1 5.8 conditional.3
  488.9 5.8 conditional.3
  494.8 5.8 conditional.3
  500.6 5.8 conditional.3
  506.5 5.8 conditional.3
  512.3 5.8 conditional.3
  518.2 5.8 conditional.3
  524.1 5.8 conditional.3
  529.9 5.8 conditional.3
  535.8 5.8 conditional.3
  541.6 5.8 conditional.3
  547.5 5.8 conditional.3
  553.3 5.8 conditional.3
  559.2 5.8 conditional.3
  565.0 5.8 conditional.3
  570.9 5.8 conditional.3
  576.7 5.8 conditional.3
  637.5 19.5 %all_to_all.5 = bf16[4,64,2048]{2,1,0:T(8,128)(2,1)S(1)} all-to-all(bf16[4,64,2048]{2,1,0:T(8,128)(2,1)S(1)} %bitcast.200), channel_id=1, replica_groups=mesh['grp'=2,'sp'=64,'tp'=4] {'tp'}, dimensions={0} | all-to-all | bytes 2097152 | tf_op jit(solution)/shard_map/all_to_all | solution.py:53
  (775 shorter events, 341.9 us)
Async XLA Ops:
  6.5 4.2 copy-start
  6.5 147.6 %all-gather.9.cloned.1.call-start = ((), (), s32[]{:S(2)}) async-start(), calls=%async_computation.3 | async-start | bytes 4259840 | tf_op jit(solution)/shard_map/all_gather | solution.py:17
  11.3 23.5 %copy-start.1 = (bf16[256,128]{1,0:T(8,128)(2,1)S(1)}, bf16[256,128]{1,0:T(8,128)(2,1)}, u32[]{:S(2)}) copy-start(bf16[256,128]{1,0:T(8,128)(2,1)} %param.32) | copy-start | bytes 196612
  11.3 23.7 %copy-start.4 = (bf16[256,64]{0,1:T(8,128)(2,1)S(1)}, bf16[256,64]{0,1:T(8,128)(2,1)}, u32[]{:S(2)}) copy-start(bf16[256,64]{0,1:T(8,128)(2,1)} %param.31) | copy-start | bytes 98308
  11.3 23.7 %copy-start.5 = (bf16[256,64]{0,1:T(8,128)(2,1)S(1)}, bf16[256,64]{0,1:T(8,128)(2,1)}, u32[]{:S(2)}) copy-start(bf16[256,64]{0,1:T(8,128)(2,1)} %param.29) | copy-start | bytes 98308
  11.3 24.4 %copy-start.2 = (bf16[256,128]{1,0:T(8,128)(2,1)S(1)}, bf16[256,128]{1,0:T(8,128)(2,1)}, u32[]{:S(2)}) copy-start(bf16[256,128]{1,0:T(8,128)(2,1)} %param.28) | copy-start | bytes 196612
  11.3 24.5 %copy-start.3 = (bf16[256,128]{1,0:T(8,128)(2,1)S(1)}, bf16[256,128]{1,0:T(8,128)(2,1)}, u32[]{:S(2)}) copy-start(bf16[256,128]{1,0:T(8,128)(2,1)} %param.30) | copy-start | bytes 196612
  11.3 24.7 %copy-start.6 = (f32[256,2]{0,1:T(2,128)S(1)}, f32[256,2]{0,1:T(2,128)}, u32[]{:S(2)}) copy-start(f32[256,2]{0,1:T(2,128)} %param.26) | copy-start | bytes 6148
  33.9 248.6 %all-gather.5.cloned.1.call-start = ((), (), s32[]{:S(2)}) async-start(), calls=%async_computation.1 | async-start | bytes 2129920 | tf_op jit(solution)/shard_map/all_gather | solution.py:277
  34.7 397.7 %all-gather.7.cloned.1.call-start = ((), (), s32[]{:S(2)}) async-start(), calls=%async_computation.2 | async-start | bytes 8519680 | tf_op jit(solution)/shard_map/all_gather | solution.py:43
  88.6 130.7 %copy-start.7 = (f32[128]{0:T(128)S(1)}, f32[128]{0:T(128)}, u32[]{:S(2)}) copy-start(f32[128]{0:T(128)} %param.27) | copy-start | bytes 1540
  447.9 187.6 %copy-start.9 = (f32[2]{0:T(128)S(1)}, f32[2]{0:T(128)}, u32[]{:S(2)}) copy-start(f32[2]{0:T(128)} %param.33) | copy-start | bytes 28
  447.9 187.7 %copy-start.8 = (f32[128]{0:T(128)S(1)}, f32[128]{0:T(128)}, u32[]{:S(2)}) copy-start(f32[128]{0:T(128)} %param.34) | copy-start | bytes 1540
Sparse Core Ops, SparseCore 0:
  34.0 120.0 all-gather.8
  156.3 126.2 all-gather.4
  284.6 147.8 all-gather.6
where the time goes:
time: 672 us; the launch traced here: 664 us
  waiting for transfers between devices  277 us (41%)
  matrix products  172 us (26%)
  other arithmetic  102 us (15%)
  blocking collectives  71.2 us (11%)
  local copies, waits for them, and re-layouts  20.7 us (3%)
  between operations  13.6 us (2%)
  loops' own time  7.26 us (1%)
    all_gather x1, waiting for transfers between devices, in_one_piece(): lax.all_gather(both, axis, axis=dim, tiled=True)  148 us
    dot_general x64, matrix products, map_update(): jnp.einsum('plew,wpd->pled', weights.astype(jnp.bfloat16), value_rows, pr...  88.7 us
    dot_general x64, matrix products, map_update(): jnp.einsum('qkgd,skd->kgqs', queries, key_rows, preferred_element_type=jn...  75.2 us
    all_gather x1, waiting for transfers between devices, carried_in(): lax.all_gather(part.astype(kind), axis)  64.9 us
    all_gather x1, waiting for transfers between devices, shards(): pieces = lax.all_gather(output_weight, 'sp', axis=2, tiled=True)  63.2 us
    select_n x64, other arithmetic, hop(): return jax.tree.map(lambda a, b: jnp.where(reached, a, b), new, before)  62.1 us
    all_gather x1, blocking collectives, carried_in(): lax.all_gather(part.astype(kind), axis)  51.6 us
    all_to_all x1, blocking collectives, summed_on_arrival(): pieces = lax.all_to_all(split_up(array, dim, size), axis, 0, 0, tiled=True)  19.5 us
  transfers between devices with their start and end apart: 3, of which 3 were waited for; matrix products, arithmetic and copies ran while one was open for 10% of the time, Pallas kernels for 0%

commit v1 on v0

--- a/solution.py
+++ b/solution.py
@@ -274,7 +274,14 @@
         recurrent_added_decay,
         recurrent_norm_gain,
     )
-    pieces = lax.all_gather(output_weight, "sp", axis=2, tiled=True)
+    nodes = jax.lax.axis_size("sp")
+    pieces = jax.lax.all_to_all(
+        jnp.tile(output_weight, [nodes if ii == 2 else 1 for ii in range(output_weight.ndim)]),
+        "sp",
+        split_axis=2,
+        concat_axis=2,
+        tiled=True,
+    )
     partial_terms = jnp.dot(
         recurrent_output, pieces[0], preferred_element_type=jnp.float32
     ) + jnp.dot(attended, pieces[1], preferred_element_type=jnp.float32)

time: 672 us -> 671 us (level)
  waiting for transfers between devices: 277 us -> 43 us
  blocking collectives: 71.2 us -> 264 us
  local copies, waits for them, and re-layouts: 20.7 us -> 51.1 us
  starting transfers between devices: 0.13 us -> 6.92 us
    all_gather x1, blocking collectives: 51.6 us -> 245 us  [carried_in(): lax.all_gather(part.astype(kind), axis)]
    all_gather x1, waiting for transfers between devices: 148 us -> 42.8 us  [in_one_piece(): lax.all_gather(both, axis, axis=dim, tiled=True)]
    all_gather x1, waiting for transfers between devices: 64.9 us -> 0.02 us  [carried_in(): lax.all_gather(part.astype(kind), axis)]
    all_gather x1 -> x0, waiting for transfers between devices: 63.2 us -> none  [shards(): pieces = lax.all_gather(output_weight, 'sp', axis=2, tiled=True)]
    another operation x4 -> x6, local copies, waits for them, and re-layouts: 0.23 us -> 14.5 us  [the longest x2 14.2 us: shards(): jnp.tile(output_weight, [nodes if ii == 2 else 1 for ii in range(output_w...]
    unnamed x26 -> x38, local copies, waits for them, and re-layouts: 8.77 us -> 19.8 us
    all_to_all x0 -> x1, starting transfers between devices: none -> 6.85 us  [shards(): jax.lax.all_to_all(jnp.tile(output_weight, [nodes if ii == 2 else 1 for i...]
  transfers between devices with their start and end apart: 3 -> 3, of which waited for: 3 -> 1; matrix products, arithmetic and copies ran while one was open for 10% -> 42% of each run, Pallas kernels for 0% -> 0%
where the time goes in v1:
time: 671 us; the launch traced here: 663 us
  blocking collectives  264 us (39%)
  matrix products  174 us (26%)
  other arithmetic  102 us (15%)
  local copies, waits for them, and re-layouts  51.1 us (8%)
  waiting for transfers between devices  43 us (6%)
  between operations  13.9 us (2%)
  loops' own time  7.32 us (1%)
  starting transfers between devices  6.92 us (1%)
    all_gather x1, blocking collectives, carried_in(): lax.all_gather(part.astype(kind), axis)  245 us
    dot_general x64, matrix products, map_update(): jnp.einsum('plew,wpd->pled', weights.astype(jnp.bfloat16), value_rows, pr...  88.7 us
    dot_general x64, matrix products, map_update(): jnp.einsum('qkgd,skd->kgqs', queries, key_rows, preferred_element_type=jn...  75.2 us
    select_n x64, other arithmetic, hop(): return jax.tree.map(lambda a, b: jnp.where(reached, a, b), new, before)  62.1 us
    all_gather x1, waiting for transfers between devices, in_one_piece(): lax.all_gather(both, axis, axis=dim, tiled=True)  42.8 us
    unnamed x38, local copies, waits for them, and re-layouts  19.8 us
    all_to_all x1, blocking collectives, summed_on_arrival(): pieces = lax.all_to_all(split_up(array, dim, size), axis, 0, 0, tiled=True)  19.3 us
    another operation x2, local copies, waits for them, and re-layouts, shards(): jnp.tile(output_weight, [nodes if ii == 2 else 1 for ii in range(output_w...  14.2 us
  transfers between devices with their start and end apart: 3, of which 1 were waited for; matrix products, arithmetic and copies ran while one was open for 42% of the time, Pallas kernels for 0%

profile of v1, /device:TPU:2016, one launch (start us, length us, event | category | flops | bytes accessed | tf_op | source)
XLA Modules:
  0.0 663.5 jit_solution(17784533058292513230)
XLA Ops:
  11.3 26.8 %while.52 = (s32[]{:T(128)}, f32[2,128,128]{2,1,0:T(8,128)S(1)}, f32[8,32,2,128]{3,1,0,2:T(8,128)}, f32[8,32,2,128]{3,2,1,0:T(2,128)S(1)}, f32[8,32,2,128]{3,2,1...) while((s32[]{:T(128)}, f32[2,128,128]{2,1,0:T(8,128)S(1)}, ...), condition=%wide.region_2.3_spmd.clone, body=%wide.region_0.2_spmd.clone.sunk | while | flops 6725635 | bytes 3267192 | solution.py:98
  39.1 14.0 %copy.209 = bf16[2,256,2048]{1,0,2:T(2,128)(2,1)} copy(bf16[2,256,2048]{1,2,0:T(8,128)(2,1)S(1)} %bitcast.201) | data formatting | bytes 4194304 | tf_op jit(solution)/shard_map/tile | solution.py:279
  53.1 6.8 %all-to-all-start = ((bf16[2,256,2048]{1,0,2:T(2,128)(2,1)}), bf16[2,256,2048]{1,0,2:T(2,128)(2,1)S(1)}, u32[]{:S(2)}, u32[]{:S(2)}) async-start(bf16[2,256,2048]{1,0,2:T(2,128)(2,1)} %copy.209), calls=%async_computation | async-start | bytes 4194304 | tf_op jit(solution)/shard_map/all_to_all | solution.py:278
  63.3 245.1 %all_gather.13 = bf16[64,2,128]{2,1,0:T(2,128)(2,1)S(1)} all-gather(bf16[1,2,128]{2,1,0:T(2,128)(2,1)S(1)} %fusion.69), channel_id=1, replica_groups=mesh['grp'=2,'sp'=64,'tp'=4] {'sp'}, dimensions={0}, use_global_device_ids=true | all-gather | bytes 33280 | tf_op jit(solution)/shard_map/all_gather | solution.py:17
  310.0 64.9 %while.53 = (s32[]{:T(128)}, f32[2,128,128]{2,1,0:T(8,128)S(1)}, s32[]{:T(128)}, bf16[64,2,128]{2,1,0:T(2,128)(2,1)S(1)}, bf16[64,2,128,128]{3,2,1,0:T(8,128)(2,1)}, /*index=5*/s32[]{:T(128)}, s32[]{:T(128)}) while((s32[]{:T(128)}, f32[2,128,128]{2,1,0:T(8,128)S(1)}, s32[]{:T(128)}, bf16[64,2,128]{2,1,0:T(2,128)(2,1)S(1)}, ...), condition=%wide.region_6.0_spmd.clone, body=%wide.region_5.6_spmd.clone.sunk | while | flops 164100 | bytes 330345 | solution.py:34
  375.3 42.8 %all-gather.4.cloned.1.call-done = bf16[16384,256]{0,1:T(8,128)(2,1)} async-done(((bf16[256,256]{0,1:T(8,128)(2,1)}), bf16[16384,256]{0,1:T(8,128)(2,1)}) %all-gather.4.cloned.1.call-update) | async-done | bytes 8388624 | tf_op jit(solution)/shard_map/all_gather | solution.py:43
  422.6 6.4 copy.214
  433.7 187.3 %while.51 = (s32[]{:T(128)}, f32[1,2,256]{2,1,0:T(2,128)S(1)}, f32[1,2,256]{2,1,0:T(2,128)S(1)}, f32[1,2,256,128]{3,2,1,0:T(8,128)S(1)}, f32[1,2,256]{2,1,0:T(2,...) while((s32[]{:T(128)}, f32[1,2,256]{2,1,0:T(2,128)S(1)}, ...), condition=%wide.region_15.16_spmd.clone, body=%wide.region_8.15_spmd.clone.sunk | while | flops 206442240 | bytes 8724921 | solution.py:232
  433.7 5.8 conditional.3
  439.6 5.8 conditional.3
  445.4 5.8 conditional.3
  451.3 5.8 conditional.3
  457.2 5.8 conditional.3
  463.0 5.8 conditional.3
  468.9 5.8 conditional.3
  474.7 5.8 conditional.3
  480.6 5.8 conditional.3
  486.4 5.8 conditional.3
  492.3 5.8 conditional.3
  498.1 5.8 conditional.3
  504.0 5.8 conditional.3
  509.8 5.8 conditional.3
  515.7 5.8 conditional.3
  521.5 5.8 conditional.3
  527.4 5.8 conditional.3
  533.2 5.8 conditional.3
  539.1 5.8 conditional.3
  544.9 5.8 conditional.3
  550.8 5.8 conditional.3
  556.6 5.8 conditional.3
  562.5 5.8 conditional.3
  636.4 19.3 %all_to_all.10 = bf16[4,64,2048]{2,1,0:T(8,128)(2,1)S(1)} all-to-all(bf16[4,64,2048]{2,1,0:T(8,128)(2,1)S(1)} %bitcast.202), channel_id=1, replica_groups=mesh['grp'=2,'sp'=64,'tp'=4] {'tp'}, dimensions={0} | all-to-all | bytes 2097152 | tf_op jit(solution)/shard_map/all_to_all | solution.py:53
  (789 shorter events, 359.9 us)
Async XLA Ops:
  6.5 4.2 copy-start.2
  6.5 303.4 %all-gather.6.cloned.1.call-start = ((), (), s32[]{:S(2)}) async-start(), calls=%async_computation.3 | async-start | bytes 4259840 | tf_op jit(solution)/shard_map/all_gather | solution.py:17
  11.3 27.5 %copy-start.8 = (bf16[2,256,32]{1,2,0:T(8,128)(2,1)S(1)}, bf16[2,256,32]{1,2,0:T(8,128)(2,1)}, u32[]{:S(2)}) copy-start(bf16[2,256,32]{1,2,0:T(8,128)(2,1)} %param.35) | copy-start | bytes 98308
  53.1 7.0 %copy-start.3 = (bf16[256,128]{1,0:T(8,128)(2,1)S(1)}, bf16[256,128]{1,0:T(8,128)(2,1)}, u32[]{:S(2)}) copy-start(bf16[256,128]{1,0:T(8,128)(2,1)} %param.32) | copy-start | bytes 196612
  53.1 7.1 %copy-start.9 = (bf16[256,64]{0,1:T(8,128)(2,1)S(1)}, bf16[256,64]{0,1:T(8,128)(2,1)}, u32[]{:S(2)}) copy-start(bf16[256,64]{0,1:T(8,128)(2,1)} %param.31) | copy-start | bytes 98308
  53.1 7.1 %copy-start.10 = (bf16[256,64]{0,1:T(8,128)(2,1)S(1)}, bf16[256,64]{0,1:T(8,128)(2,1)}, u32[]{:S(2)}) copy-start(bf16[256,64]{0,1:T(8,128)(2,1)} %param.29) | copy-start | bytes 98308
  53.1 7.9 %copy-start.4 = (bf16[256,128]{1,0:T(8,128)(2,1)S(1)}, bf16[256,128]{1,0:T(8,128)(2,1)}, u32[]{:S(2)}) copy-start(bf16[256,128]{1,0:T(8,128)(2,1)} %param.28) | copy-start | bytes 196612
  53.1 8.6 %copy-start.5 = (bf16[256,128]{1,0:T(8,128)(2,1)S(1)}, bf16[256,128]{1,0:T(8,128)(2,1)}, u32[]{:S(2)}) copy-start(bf16[256,128]{1,0:T(8,128)(2,1)} %param.30) | copy-start | bytes 196612
  53.1 9.3 %copy-start.11 = (f32[256,2]{0,1:T(2,128)S(1)}, f32[256,2]{0,1:T(2,128)}, u32[]{:S(2)}) copy-start(f32[256,2]{0,1:T(2,128)} %param.26) | copy-start | bytes 6148
  53.1 568.3 %all-to-all-start = ((bf16[2,256,2048]{1,0,2:T(2,128)(2,1)}), bf16[2,256,2048]{1,0,2:T(2,128)(2,1)S(1)}, u32[]{:S(2)}, u32[]{:S(2)}) async-start(bf16[2,256,2048]{1,0,2:T(2,128)(2,1)} %copy.209), calls=%async_computation | async-start | bytes 4194304 | tf_op jit(solution)/shard_map/all_to_all | solution.py:278
  60.0 358.2 %all-gather.4.cloned.1.call-start = ((), (), s32[]{:S(2)}) async-start(), calls=%async_computation.2 | async-start | bytes 8519680 | tf_op jit(solution)/shard_map/all_gather | solution.py:43
  308.4 66.8 %copy-start.12 = (f32[128]{0:T(128)S(1)}, f32[128]{0:T(128)}, u32[]{:S(2)}) copy-start(f32[128]{0:T(128)} %param.27) | copy-start | bytes 1540
  429.0 4.7 copy-start.6
  429.0 4.7 copy-start.7
  433.7 187.6 %copy-start.14 = (f32[2]{0:T(128)S(1)}, f32[2]{0:T(128)}, u32[]{:S(2)}) copy-start(f32[2]{0:T(128)} %param.33) | copy-start | bytes 28
  625.6 4.7 copy-start
  634.7 0.7 copy-start.13
  634.7 1.2 copy-start.1
Sparse Core Ops, SparseCore 0:
  38.9 218.6 all-gather.5
  259.6 158.4 all-gather.3
